TPU v7x, 256 devices: a whole 4x4x8 slice. The times are simulated.
256 devices in a mesh: ep: 128 (over z, y, x), tp: 2 (over core).
Axes of the slice: x: 4, y: 4, z: 8, core: 2. Of those that a mesh axis runs over, the one named last changes fastest.
Arguments:
- tokens: bfloat16 [512, 2048], P('ep'), may hold values from -6 to 6
- lengths: int32 [512], P('ep'), may hold values from 1 to 1024
- cache_keys: bfloat16 [512, 1024, 512], P('ep', None, 'tp'), may hold values from -640 to 640
- cache_values: bfloat16 [512, 1024, 512], P('ep', None, 'tp'), may hold values from -6 to 6
- norm0_gain: float32 [2048], replicated, may hold values from 0.1 to 1.9
- query_weight: bfloat16 [2048, 1536], P('ep', 'tp'), may hold values from -0.125 to 0.125
- key_weight: bfloat16 [2048, 512], P('ep', 'tp'), may hold values from -0.21875 to 0.21875
- value_weight: bfloat16 [2048, 512], P('ep', 'tp'), may hold values from -0.125 to 0.125
- mix_lambda: float32 [6], P('tp'), may hold values from 0.3 to 0.8
- head_gain: float32 [256], replicated, may hold values from 0.1 to 1.9
- out_weight: bfloat16 [1536, 2048], P('tp', 'ep'), may hold values from -0.15625 to 0.15625
- norm1_gain: float32 [2048], replicated, may hold values from 0.1 to 1.9
- group_ids: int32 [512], P('ep'), may hold values from 0 to 31, as said below
- member_ids: int32 [512, 2], P('ep'), may hold values from 0 to 3, as said below
- group_weight: float32 [512], P('ep'), may hold values from 0.3 to 1
- member_weights: float32 [512, 2], P('ep'), may hold values from 0.2 to 1
- expert_gate: bfloat16 [128, 2048, 512], P('ep', None, 'tp'), may hold values from -0.125 to 0.125
- expert_up: bfloat16 [128, 2048, 512], P('ep', None, 'tp'), may hold values from -0.125 to 0.125
- expert_down: bfloat16 [128, 512, 2048], P('ep', 'tp'), may hold values from -0.25 to 0.25
- norm2_gain: float32 [2048], P('tp'), may hold values from 0.1 to 1.9
Outputs:
- result: bfloat16 [512, 2048], P('ep', 'tp')
Inputs may be any that keep to these rules, and one draw needn't show every extreme that they name: `group_ids`: every group is named by exactly 16 tokens; the 4 tokens of one device name different groups. `member_ids`: A token's 2 members are different; no expert is used by more than 16 tokens, and some expert by exactly 16.
All inputs are finite; a program needn't handle non-finite values.
Results may differ from a plain program's by a relative error of at most 0.015.
Values may be sent and summed in bfloat16 or wider, within the bound.
No kernel may reach another device: no remote copies, remote signals or barrier semaphores. Data moves between devices by JAX's collectives and lax.ppermute only.
A program may use at most 64 MiB of HBM per device.

v0:
```python
import jax
import jax.numpy as jnp
from jax import lax
from jax.sharding import Mesh
from jax.sharding import PartitionSpec as P

EPG = 4
EP = ("z", "y", "x")
ROW = ("y", "x")
ALPHA = 2.0**0.25
EPS = 1e-05


def swap(array, axis):
    return lax.all_to_all(array, axis, 0, 0, tiled=True)


def to_all(array, axis):
    return swap(jnp.broadcast_to(array[None], (lax.axis_size(axis), *array.shape)), axis)


def layer_norm(values, gain):
    mean = jnp.mean(values, -1, keepdims=True)
    spread = jnp.mean(jnp.square(values - mean), -1, keepdims=True)
    return (values - mean) * lax.rsqrt(spread + EPS) * gain


def attend(queries, new_keys, new_values, cache_keys, cache_values, lengths, mix_lambda, head_gain):
    seqs = queries.shape[0]
    span = cache_keys.shape[1]
    vwidth = head_gain.shape[0]
    kv_local = cache_values.shape[2] // vwidth
    hwidth = cache_keys.shape[2] // (2 * kv_local)
    heads_local = mix_lambda.shape[0]
    group = heads_local // kv_local
    query_grid = queries.reshape(seqs, kv_local, group, 2, hwidth)
    cached_keys = cache_keys.reshape(seqs, span, kv_local, 2, hwidth)
    fresh_keys = new_keys.reshape(seqs, kv_local, 2, hwidth)
    cached_values = cache_values.reshape(seqs, span, kv_local, vwidth)
    fresh_values = new_values.reshape(seqs, kv_local, vwidth)
    valid = (jnp.arange(span, dtype=jnp.int32)[None, :] < lengths[:, None])[:, None, None, :]
    scale = hwidth ** (-0.5)
    maps = []
    for which in range(2):
        cached = (
            jnp.einsum(
                "sghd,scgd->sghc",
                query_grid[:, :, :, which],
                cached_keys[:, :, :, which],
                preferred_element_type=jnp.float32,
            )
            * scale
        )
        fresh = (
            jnp.einsum(
                "sghd,sgd->sgh",
                query_grid[:, :, :, which],
                fresh_keys[:, :, which],
                preferred_element_type=jnp.float32,
            )
            * scale
        )
        highest = jnp.maximum(jnp.max(jnp.where(valid, cached, -1e30), -1), fresh)
        spread = jnp.where(valid, jnp.exp(cached - highest[..., None]), 0.0)
        itself = jnp.exp(fresh - highest)
        total = jnp.sum(spread, -1) + itself
        maps.append((spread / total[..., None], itself / total))
    lambdas = mix_lambda.reshape(1, kv_local, group)
    cached_weight = (maps[0][0] - lambdas[..., None] * maps[1][0]).astype(jnp.bfloat16)
    fresh_weight = (maps[0][1] - lambdas * maps[1][1]).astype(jnp.bfloat16)
    head_out = jnp.einsum(
        "sghc,scgv->sghv", cached_weight, cached_values, preferred_element_type=jnp.float32
    )
    head_out = (
        head_out
        + fresh_weight.astype(jnp.float32)[..., None]
        * fresh_values.astype(jnp.float32)[:, :, None, :]
    )
    head_out = (
        head_out * lax.rsqrt(jnp.mean(head_out * head_out, -1, keepdims=True) + EPS) * head_gain
    )
    return head_out.astype(jnp.bfloat16).reshape(seqs, heads_local * vwidth)


def shards(
    tokens,
    lengths,
    cache_keys,
    cache_values,
    norm0_gain,
    query_weight,
    key_weight,
    value_weight,
    mix_lambda,
    head_gain,
    out_weight,
    norm1_gain,
    group_ids,
    member_ids,
    group_weight,
    member_weights,
    expert_gate,
    expert_up,
    expert_down,
    norm2_gain,
):
    seqs, width = tokens.shape
    deep = lax.axis_size("z")
    experts = lax.axis_size(EP)
    halves = lax.axis_size("tp")
    half = width // halves
    block = width // deep
    query_cols = query_weight.shape[1]
    key_cols = key_weight.shape[1]
    value_cols = value_weight.shape[1]
    proj_cols = query_cols + key_cols + value_cols
    expert_ids = group_ids[:, None] * EPG + member_ids
    share = group_weight[:, None] * member_weights
    own_weights = jnp.concatenate((query_weight, key_weight, value_weight, out_weight.T), 1)
    weights = to_all(own_weights, ROW).reshape(block, -1)
    weight_in = weights[:, :proj_cols]
    weight_out = weights[:, proj_cols:]
    normed = layer_norm(tokens.astype(jnp.float32), norm0_gain).astype(jnp.bfloat16)
    columns = swap(normed.reshape(seqs, deep, block).transpose(1, 0, 2), "z")
    partial = jnp.dot(
        columns.reshape(deep * seqs, block), weight_in, preferred_element_type=jnp.float32
    )
    projected = jnp.sum(swap(partial.reshape(deep, seqs, proj_cols), "z"), 0).astype(jnp.bfloat16)
    queries = projected[:, :query_cols]
    new_keys = projected[:, query_cols : query_cols + key_cols]
    new_values = projected[:, query_cols + key_cols :]
    attended = attend(
        queries, new_keys, new_values, cache_keys, cache_values, lengths, mix_lambda, head_gain
    )
    everyone = to_all(attended, "z").reshape(deep * seqs, -1)
    partial_mix = lax.dot_general(
        everyone, weight_out, (((1,), (1,)), ((), ())), preferred_element_type=jnp.float32
    ).astype(jnp.bfloat16)
    doubled = jnp.broadcast_to(
        partial_mix.reshape(deep, 1, seqs, block), (deep, halves, seqs, block)
    )
    back = swap(doubled.reshape(deep * halves, seqs, block), ("z", "tp"))
    mix = jnp.sum(back.astype(jnp.float32).reshape(deep, halves, seqs, block), 1)
    mix = mix.transpose(1, 0, 2).reshape(seqs, width).astype(jnp.bfloat16)
    stream = (ALPHA * normed.astype(jnp.float32) + mix.astype(jnp.float32)).astype(jnp.bfloat16)
    settled = layer_norm(stream.astype(jnp.float32), norm1_gain).astype(jnp.bfloat16)
    targets = lax.iota(jnp.int32, experts)
    select = jnp.any(expert_ids[None, :, :] == targets[:, None, None], 2)
    tiles = settled.reshape(1, seqs, width // 128, 128)
    sending = jnp.sum(
        jnp.where(select[:, :, None, None], tiles, jnp.zeros_like(tiles)).astype(jnp.float32), 1
    ).astype(jnp.bfloat16)
    rows = swap(sending, EP).reshape(experts, width)
    gate = jnp.dot(rows, expert_gate[0], preferred_element_type=jnp.float32)
    upward = jnp.dot(rows, expert_up[0], preferred_element_type=jnp.float32)
    hidden = (jax.nn.silu(gate) * upward).astype(jnp.bfloat16)
    output = jnp.dot(hidden, expert_down[0], preferred_element_type=jnp.float32)
    output = output.astype(jnp.bfloat16).reshape(experts * halves, half // 128, 128)
    returned = swap(output, EP + ("tp",)).reshape(experts, halves, half // 128, 128)
    both = jnp.sum(returned.astype(jnp.float32), 1)
    combine = jnp.sum(
        jnp.where(expert_ids[:, :, None] == targets[None, None, :], share[:, :, None], 0.0), 1
    )
    routed = jnp.sum(combine[:, :, None, None] * both[None], 1).reshape(seqs, half)
    own = lax.dynamic_slice_in_dim(settled, lax.axis_index("tp") * half, half, 1)
    mixed = ALPHA * own.astype(jnp.float32) + routed
    sums = lax.psum(jnp.stack((jnp.sum(mixed, 1), jnp.sum(mixed * mixed, 1))), "tp")
    mean = sums[0] / width
    spread = sums[1] / width - mean * mean
    result = (mixed - mean[:, None]) * lax.rsqrt(spread[:, None] + EPS) * norm2_gain
    return result.astype(jnp.bfloat16)


def solution(mesh):
    torus = Mesh(mesh.devices.reshape(8, 4, 4, mesh.shape["tp"]), ("z", "y", "x", "tp"))
    return jax.shard_map(
        shards,
        mesh=torus,
        in_specs=(
            P(EP, None),
            P(EP),
            P(EP, None, "tp"),
            P(EP, None, "tp"),
            P(),
            P(EP, "tp"),
            P(EP, "tp"),
            P(EP, "tp"),
            P("tp"),
            P(),
            P("tp", EP),
            P(),
            P(EP),
            P(EP, None),
            P(EP),
            P(EP, None),
            P(EP, None, "tp"),
            P(EP, None, "tp"),
            P(EP, "tp", None),
            P("tp"),
        ),
        out_specs=P(EP, "tp"),
        check_vma=False,
    )
```

profile of v0, /device:TPU:1, one launch (start us, length us, event | category | flops | bytes accessed | tf_op | source)
XLA Modules:
  0.0 149.5 jit_solution(3451434910616258476)
XLA Ops:
  0.0 0.0 copy-start
  0.0 1.0 convert_reduce_fusion.2
  1.0 0.9 fusion.31
  1.9 1.4 fusion.33
  3.3 9.0 %all-to-all-start = ((bf16[8,4,256]{2,1,0:T(4,128)(2,1)}), bf16[8,4,256]{2,1,0:T(4,128)(2,1)S(1)}, u32[]{:S(2)}, u32[]{:S(2)}) async-start(bf16[8,4,256]{2,1,0:T(4,128)(2,1)} %bitcast.1), calls=%async_computation | async-start | bytes 32768 | tf_op jit(solution)/shard_map/all_to_all | solution.py:15
  12.3 0.8 pad_maximum_fusion
  13.1 5.8 %all-to-all-done = bf16[8,4,256]{2,1,0:T(4,128)(2,1)S(1)} async-done(((bf16[8,4,256]{2,1,0:T(4,128)(2,1)}), bf16[8,4,256]{2,1,0:T(4,128)(2,1)S(1)}, u32[]{:S(2)}, u32[]{:S(2)}) %all-to-all-start) | async-done | bytes 16416 | tf_op jit(solution)/shard_map/all_to_all | solution.py:15
  19.0 0.1 broadcast_in_dim.116
  19.1 22.2 %all_to_all.35 = bf16[16,16,2048]{2,1,0:T(8,128)(2,1)S(1)} all-to-all(bf16[16,16,2048]{2,1,0:T(8,128)(2,1)S(1)} %broadcast_in_dim.116), channel_id=1, replica_groups=mesh['z'=8,'y'=4,'x'=4,'tp'=2] {'y','x'}, dimensions={0} | all-to-all | bytes 2097152 | tf_op jit(solution)/shard_map/all_to_all | solution.py:15
  41.3 0.9 fusion.6
  42.2 3.4 %all-to-all-start.2 = ((f32[8,4,1280]{2,1,0:T(4,128)}), f32[8,4,1280]{2,1,0:T(4,128)S(1)}, u32[]{:S(2)}, u32[]{:S(2)}) async-start(f32[8,4,1280]{2,1,0:T(4,128)} %fusion.6), calls=%async_computation.2 | async-start | bytes 327680 | tf_op jit(solution)/shard_map/all_to_all | solution.py:15
  45.5 0.0 copy-done.11
  45.6 0.0 copy-start.8
  45.6 4.0 %copy.53 = bf16[4,1024,256]{1,2,0:T(8,128)(2,1)} copy(bf16[4,1024,256]{2,1,0:T(8,128)(2,1)} %param.22) | data formatting | bytes 4194304 | tf_op args[2]
  49.6 0.0 copy-done.8
  49.6 0.1 iota_compare_fusion
  49.7 4.1 %all-to-all-done.2 = f32[8,4,1280]{2,1,0:T(4,128)S(1)} async-done(((f32[8,4,1280]{2,1,0:T(4,128)}), f32[8,4,1280]{2,1,0:T(4,128)S(1)}, u32[]{:S(2)}, u32[]{:S(2)}) %all-to-all-start.2) | async-done | bytes 163872 | tf_op jit(solution)/shard_map/all_to_all | solution.py:15
  53.8 0.1 fusion.43
  53.9 1.6 %select_reduce_fusion.2 = (f32[4,3]{1,0:T(4,128)S(1)}, f32[4,3,1024]{2,1,0:T(4,128)S(1)}) fusion(pred[4,1024]{1,0:T(4,128)(4,1)S(1)} %iota_compare_fusion, bf16[4,1024,1,2,128]{1,4,3,0,2:T(8,128)(2,1)} %bitcast.111, bf16[4,1,3,1,128]{4,0,3,2,1:T(4,128)(2,1)S(1)} %get-tuple-element.17), kind=kOutput, calls=%fused_computation.34 | convolution fusion | flops 3182580 | bytes 1104944 | tf_op jit(solution)/shard_map/sghd,scgd->sghc/dot_general | solution.py:46
  55.5 0.1 fusion.44
  55.6 1.6 %fusion.21 = (f32[4,3]{1,0:T(4,128)S(1)}, f32[4,3]{1,0:T(4,128)S(1)}, f32[4,3,1024]{2,1,0:T(4,128)S(1)}) fusion(f32[4,3,1024]{2,1,0:T(4,128)S(1)} %get-tuple-element.21, f32[4,3]{1,0:T(4,128)S(1)} %multiply_maximum_fusion.1, pred[4,1024]{1,0:T(4,128)(4,1)S(1)} %iota_compare_fusion, bf16[4,1024,1,2,128]{1,4,3,0,2:T(8,128)(2,1)} %bitcast.112, ...), kind=kOutput, calls=%fused_computation.36 | convolution fusion | flops 3219432 | bytes 1154192 | tf_op jit(solution)/shard_map/sghd,scgd->sghc/dot_general | solution.py:46
  57.2 0.2 fusion.22
  57.4 0.0 copy-done.9
  57.4 0.0 copy-done
  57.4 0.5 multiply_reduce_fusion.2
  58.0 0.0 copy-done.5
  58.0 0.1 fusion.41
  58.1 0.6 broadcast_in_dim.120
  58.7 3.3 %all-to-all-start.3 = ((bf16[8,4,768]{2,1,0:T(4,128)(2,1)}), bf16[8,4,768]{2,1,0:T(4,128)(2,1)S(1)}, u32[]{:S(2)}, u32[]{:S(2)}) async-start(bf16[8,4,768]{2,1,0:T(4,128)(2,1)} %broadcast_in_dim.120), calls=%async_computation.3 | async-start | bytes 98304 | tf_op jit(solution)/shard_map/all_to_all | solution.py:15
  62.1 0.0 copy-done.6
  62.1 6.9 %all-to-all-done.3 = bf16[8,4,768]{2,1,0:T(4,128)(2,1)S(1)} async-done(((bf16[8,4,768]{2,1,0:T(4,128)(2,1)}), bf16[8,4,768]{2,1,0:T(4,128)(2,1)S(1)}, u32[]{:S(2)}, u32[]{:S(2)}) %all-to-all-start.3) | async-done | bytes 49184 | tf_op jit(solution)/shard_map/all_to_all | solution.py:15
  69.1 0.2 convolution_convert_fusion.1
  69.3 0.1 broadcast_in_dim.121
  69.3 0.6 broadcast_in_dim.122
  70.0 8.5 %all-to-all-start.4 = ((bf16[16,4,256]{2,1,0:T(4,128)(2,1)}), bf16[16,4,256]{2,1,0:T(4,128)(2,1)S(1)}, u32[]{:S(2)}, u32[]{:S(2)}) async-start(bf16[16,4,256]{2,1,0:T(4,128)(2,1)} %bitcast.20), calls=%async_computation.4 | async-start | bytes 65536 | tf_op jit(solution)/shard_map/all_to_all | solution.py:15
  78.5 0.1 fusion.42
  78.6 0.1 copy.58
  78.7 7.3 %all-to-all-done.4 = bf16[16,4,256]{2,1,0:T(4,128)(2,1)S(1)} async-done(((bf16[16,4,256]{2,1,0:T(4,128)(2,1)}), bf16[16,4,256]{2,1,0:T(4,128)(2,1)S(1)}, u32[]{:S(2)}, u32[]{:S(2)}) %all-to-all-start.4) | async-done | bytes 32800 | tf_op jit(solution)/shard_map/all_to_all | solution.py:15
  86.0 0.0 copy-done.1
  86.0 0.0 copy-done.2
  86.1 0.2 convert_reduce_fusion.1
  86.3 0.2 fusion.28
  86.5 0.0 copy-done.3
  86.5 0.1 fusion.59
  86.6 1.0 select_reduce_fusion
  87.6 24.7 %all_to_all.36 = bf16[128,16,128]{2,1,0:T(8,128)(2,1)S(1)} all-to-all(bf16[128,16,128]{2,1,0:T(8,128)(2,1)S(1)} %select_reduce_fusion), channel_id=1, replica_groups=mesh['z'=8,'y'=4,'x'=4,'tp'=2] {'z','y','x'}, dimensions={0} | all-to-all | bytes 1048576 | tf_op jit(solution)/shard_map/all_to_all | solution.py:15
  112.3 1.5 %fusion.4 = f32[128,256]{1,0:T(8,128)S(1)} fusion(bf16[1,2048,256]{2,1,0:T(8,128)(2,1)} %param.36, bf16[16,8,16,128]{3,2,1,0:T(8,128)(2,1)S(1)} %bitcast.107), kind=kOutput, calls=%fused_computation.14 | convolution fusion | flops 134217728 | bytes 1703936 | tf_op jit(solution)/shard_map/dot_general | solution.py:154
  113.8 0.0 copy-start.7
  113.8 0.0 copy-start.10
  113.8 2.3 %convolution_convert_fusion = bf16[128,2048]{1,0:T(8,128)(2,1)S(1)} fusion(bf16[1,256,2048]{2,1,0:T(8,128)(2,1)} %param.38, bf16[1,2048,256]{2,1,0:T(8,128)(2,1)} %param.37, bf16[16,8,16,128]{3,2,1,0:T(8,128)(2,1)S(1)} %bitcast.108, f32[128,256]{1,0:T(8,128)S(1)} %fusion.4), kind=kOutput, calls=%fused_computation | convolution fusion | flops 268894208 | bytes 3276800 | tf_op jit(solution)/shard_map/dot_general | solution.py:157
  116.1 0.0 copy-start.4
  116.2 1.0 reshape.284
  117.2 7.5 %all-to-all-start.6 = ((bf16[256,8,128]{2,1,0:T(8,128)(2,1)}), bf16[256,8,128]{2,1,0:T(8,128)(2,1)S(1)}, u32[]{:S(2)}, u32[]{:S(2)}) async-start(bf16[256,8,128]{2,1,0:T(8,128)(2,1)} %reshape.284), calls=%async_computation.6 | async-start | bytes 1048576 | tf_op jit(solution)/shard_map/all_to_all | solution.py:15
  124.7 0.0 copy-done.7
  124.7 0.0 copy-done.10
  124.8 0.1 select_reduce_fusion.3
  124.8 0.1 fusion.30
  124.9 19.8 %all-to-all-done.6 = bf16[256,8,128]{2,1,0:T(8,128)(2,1)S(1)} async-done(((bf16[256,8,128]{2,1,0:T(8,128)(2,1)}), bf16[256,8,128]{2,1,0:T(8,128)(2,1)S(1)}, u32[]{:S(2)}, u32[]{:S(2)}) %all-to-all-start.6) | async-done | bytes 524320 | tf_op jit(solution)/shard_map/all_to_all | solution.py:15
  144.7 0.1 convert_reduce_fusion
  144.9 0.7 multiply_reduce_fusion
  145.6 0.2 fusion.54
  145.8 3.0 %psum.7 = f32[2,4]{1,0:T(2,128)S(1)} all-reduce(f32[2,4]{1,0:T(2,128)S(1)} %pad_maximum_fusion.1), channel_id=1, replica_groups=mesh['z'=8,'y'=4,'x'=4,'tp'=2] {'tp'}, use_global_device_ids=true, to_apply=%region_18.19 | all-reduce | flops 8 | bytes 64 | tf_op jit(solution)/shard_map/psum | solution.py:167
  148.8 0.0 copy-done.4
  148.8 0.7 multiply_convert_fusion
  (32 shorter events, 0.2 us)
Async XLA Ops:
  0.0 57.4 %copy-start = (bf16[4,1024,256]{2,1,0:T(8,128)(2,1)S(1)}, bf16[4,1024,256]{2,1,0:T(8,128)(2,1)}, u32[]{:S(2)}) copy-start(bf16[4,1024,256]{2,1,0:T(8,128)(2,1)} %param.23) | copy-start | bytes 6291460
  3.3 15.6 %all-to-all-start = ((bf16[8,4,256]{2,1,0:T(4,128)(2,1)}), bf16[8,4,256]{2,1,0:T(4,128)(2,1)S(1)}, u32[]{:S(2)}, u32[]{:S(2)}) async-start(bf16[8,4,256]{2,1,0:T(4,128)(2,1)} %bitcast.1), calls=%async_computation | async-start | bytes 32768 | tf_op jit(solution)/shard_map/all_to_all | solution.py:15
  13.1 32.4 %copy-start.11 = (s32[4]{0:T(128)S(1)}, s32[4]{0:T(128)}, u32[]{:S(2)}) copy-start(s32[4]{0:T(128)} %param.32) | copy-start | bytes 52
  42.2 11.6 %all-to-all-start.2 = ((f32[8,4,1280]{2,1,0:T(4,128)}), f32[8,4,1280]{2,1,0:T(4,128)S(1)}, u32[]{:S(2)}, u32[]{:S(2)}) async-start(f32[8,4,1280]{2,1,0:T(4,128)} %fusion.6), calls=%async_computation.2 | async-start | bytes 327680 | tf_op jit(solution)/shard_map/all_to_all | solution.py:15
  45.6 4.0 %copy-start.8 = (s32[4]{0:T(128)S(1)}, s32[4]{0:T(128)}, u32[]{:S(2)}) copy-start(s32[4]{0:T(128)} %param.21) | copy-start | bytes 52
  49.6 7.8 %copy-start.9 = (f32[3]{0:T(128)S(1)}, f32[3]{0:T(128)}, u32[]{:S(2)}) copy-start(f32[3]{0:T(128)} %param.28) | copy-start | bytes 40
  55.5 2.5 %copy-start.5 = (f32[256]{0:T(256)S(1)}, f32[256]{0:T(256)}, u32[]{:S(2)}) copy-start(f32[256]{0:T(256)} %param.29) | copy-start | bytes 3076
  55.5 6.6 %copy-start.6 = (s32[4,2]{0,1:T(2,128)S(1)}, s32[4,2]{0,1:T(2,128)}, u32[]{:S(2)}) copy-start(s32[4,2]{0,1:T(2,128)} %param.33) | copy-start | bytes 100
  57.2 28.8 %copy-start.1 = (bf16[4,2048]{1,0:T(4,128)(2,1)S(1)}, bf16[4,2048]{1,0:T(4,128)(2,1)}, u32[]{:S(2)}) copy-start(bf16[4,2048]{1,0:T(4,128)(2,1)} %param.20) | copy-start | bytes 49156
  57.2 28.8 %copy-start.2 = (f32[2048]{0:T(1024)S(1)}, f32[2048]{0:T(1024)}, u32[]{:S(2)}) copy-start(f32[2048]{0:T(1024)} %param.24) | copy-start | bytes 24580
  57.2 29.3 %copy-start.3 = (f32[2048]{0:T(1024)S(1)}, f32[2048]{0:T(1024)}, u32[]{:S(2)}) copy-start(f32[2048]{0:T(1024)} %param.31) | copy-start | bytes 24580
  58.7 10.3 %all-to-all-start.3 = ((bf16[8,4,768]{2,1,0:T(4,128)(2,1)}), bf16[8,4,768]{2,1,0:T(4,128)(2,1)S(1)}, u32[]{:S(2)}, u32[]{:S(2)}) async-start(bf16[8,4,768]{2,1,0:T(4,128)(2,1)} %broadcast_in_dim.120), calls=%async_computation.3 | async-start | bytes 98304 | tf_op jit(solution)/shard_map/all_to_all | solution.py:15
  70.0 16.0 %all-to-all-start.4 = ((bf16[16,4,256]{2,1,0:T(4,128)(2,1)}), bf16[16,4,256]{2,1,0:T(4,128)(2,1)S(1)}, u32[]{:S(2)}, u32[]{:S(2)}) async-start(bf16[16,4,256]{2,1,0:T(4,128)(2,1)} %bitcast.20), calls=%async_computation.4 | async-start | bytes 65536 | tf_op jit(solution)/shard_map/all_to_all | solution.py:15
  113.8 10.9 %copy-start.7 = (f32[4,2]{0,1:T(2,128)S(1)}, f32[4,2]{0,1:T(2,128)}, u32[]{:S(2)}) copy-start(f32[4,2]{0,1:T(2,128)} %param.35) | copy-start | bytes 100
  113.8 10.9 %copy-start.10 = (f32[4]{0:T(128)S(1)}, f32[4]{0:T(128)}, u32[]{:S(2)}) copy-start(f32[4]{0:T(128)} %param.34) | copy-start | bytes 52
  116.1 32.7 %copy-start.4 = (f32[1024]{0:T(1024)S(1)}, f32[1024]{0:T(1024)}, u32[]{:S(2)}) copy-start(f32[1024]{0:T(1024)} %param.39) | copy-start | bytes 12292
  117.2 27.6 %all-to-all-start.6 = ((bf16[256,8,128]{2,1,0:T(8,128)(2,1)}), bf16[256,8,128]{2,1,0:T(8,128)(2,1)S(1)}, u32[]{:S(2)}, u32[]{:S(2)}) async-start(bf16[256,8,128]{2,1,0:T(8,128)(2,1)} %reshape.284), calls=%async_computation.6 | async-start | bytes 1048576 | tf_op jit(solution)/shard_map/all_to_all | solution.py:15
where the time goes:
time: 150 us
  blocking collectives  49.9 us (33%)
  waiting for transfers between devices  43.9 us (29%)
  starting transfers between devices  31.8 us (21%)
  matrix products  8.88 us (6%)
  other arithmetic  8 us (5%)
  local copies, waits for them, and re-layouts  6.71 us (4%)
    all_to_all x2, blocking collectives, swap(): return lax.all_to_all(array, axis, 0, 0, tiled=True)  46.9 us
    all_to_all x5, waiting for transfers between devices, swap(): return lax.all_to_all(array, axis, 0, 0, tiled=True)  43.9 us
    all_to_all x5, starting transfers between devices, swap(): return lax.all_to_all(array, axis, 0, 0, tiled=True)  31.8 us
    unnamed x28, local copies, waits for them, and re-layouts  4.09 us
    dot_general x2, matrix products, attend(): jnp.einsum('sghd,scgd->sghc', query_grid[:, :, :, which], cached_keys[:,...  3.14 us
    psum x1, blocking collectives, shards(): lax.psum(jnp.stack((jnp.sum(mixed, 1), jnp.sum(mixed * mixed, 1))), 'tp')  3.04 us
  transfers between devices with their start and end apart: 5, of which 5 were waited for; matrix products, arithmetic and copies ran while one was open for 4% of the time, Pallas kernels for 0%

commit v1 on v0

--- a/solution.py
+++ b/solution.py
@@ -164,7 +164,11 @@
     routed = jnp.sum(combine[:, :, None, None] * both[None], 1).reshape(seqs, half)
     own = lax.dynamic_slice_in_dim(settled, lax.axis_index("tp") * half, half, 1)
     mixed = ALPHA * own.astype(jnp.float32) + routed
-    sums = lax.psum(jnp.stack((jnp.sum(mixed, 1), jnp.sum(mixed * mixed, 1))), "tp")
+
+    def render_ports(my_data, across):
+        return jnp.sum(lax.all_gather(my_data, across), axis=0)
+
+    sums = render_ports(jnp.stack((jnp.sum(mixed, 1), jnp.sum(mixed * mixed, 1))), "tp")
     mean = sums[0] / width
     spread = sums[1] / width - mean * mean
     result = (mixed - mean[:, None]) * lax.rsqrt(spread[:, None] + EPS) * norm2_gain

time: 150 us -> 150 us (level)
    psum x1 -> x0, blocking collectives: 3.04 us -> none  [shards(): lax.psum(jnp.stack((jnp.sum(mixed, 1), jnp.sum(mixed * mixed, 1))), 'tp')]
    all_gather x0 -> x1, blocking collectives: none -> 2.38 us  [render_ports(): return jnp.sum(lax.all_gather(my_data, across), axis=0)]
where the time goes in v1:
time: 150 us; the launch traced here: 149 us
  blocking collectives  49.2 us (33%)
  waiting for transfers between devices  43.9 us (29%)
  starting transfers between devices  31.8 us (21%)
  matrix products  8.88 us (6%)
  other arithmetic  8.02 us (5%)
  local copies, waits for them, and re-layouts  6.71 us (4%)
    all_to_all x2, blocking collectives, swap(): return lax.all_to_all(array, axis, 0, 0, tiled=True)  46.9 us
    all_to_all x5, waiting for transfers between devices, swap(): return lax.all_to_all(array, axis, 0, 0, tiled=True)  43.9 us
    all_to_all x5, starting transfers between devices, swap(): return lax.all_to_all(array, axis, 0, 0, tiled=True)  31.8 us
    unnamed x28, local copies, waits for them, and re-layouts  4.09 us
    dot_general x2, matrix products, attend(): jnp.einsum('sghd,scgd->sghc', query_grid[:, :, :, which], cached_keys[:,...  3.14 us
  transfers between devices with their start and end apart: 5, of which 5 were waited for; matrix products, arithmetic and copies ran while one was open for 4% of the time, Pallas kernels for 0%

profile of v1, /device:TPU:1, one launch (start us, length us, event | category | flops | bytes accessed | tf_op | source)
XLA Modules:
  0.0 148.9 jit_solution(13023714836493301443)
XLA Ops:
  0.0 0.0 copy-start
  0.0 1.0 convert_reduce_fusion.2
  1.0 0.9 fusion.31
  1.9 1.4 fusion.33
  3.3 9.0 %all-to-all-start = ((bf16[8,4,256]{2,1,0:T(4,128)(2,1)}), bf16[8,4,256]{2,1,0:T(4,128)(2,1)S(1)}, u32[]{:S(2)}, u32[]{:S(2)}) async-start(bf16[8,4,256]{2,1,0:T(4,128)(2,1)} %bitcast.1), calls=%async_computation | async-start | bytes 32768 | tf_op jit(solution)/shard_map/all_to_all | solution.py:15
  12.3 0.8 pad_maximum_fusion
  13.1 5.8 %all-to-all-done = bf16[8,4,256]{2,1,0:T(4,128)(2,1)S(1)} async-done(((bf16[8,4,256]{2,1,0:T(4,128)(2,1)}), bf16[8,4,256]{2,1,0:T(4,128)(2,1)S(1)}, u32[]{:S(2)}, u32[]{:S(2)}) %all-to-all-start) | async-done | bytes 16416 | tf_op jit(solution)/shard_map/all_to_all | solution.py:15
  19.0 0.1 broadcast_in_dim.116
  19.1 22.2 %all_to_all.35 = bf16[16,16,2048]{2,1,0:T(8,128)(2,1)S(1)} all-to-all(bf16[16,16,2048]{2,1,0:T(8,128)(2,1)S(1)} %broadcast_in_dim.116), channel_id=1, replica_groups=mesh['z'=8,'y'=4,'x'=4,'tp'=2] {'y','x'}, dimensions={0} | all-to-all | bytes 2097152 | tf_op jit(solution)/shard_map/all_to_all | solution.py:15
  41.3 0.9 fusion.6
  42.2 3.4 %all-to-all-start.2 = ((f32[8,4,1280]{2,1,0:T(4,128)}), f32[8,4,1280]{2,1,0:T(4,128)S(1)}, u32[]{:S(2)}, u32[]{:S(2)}) async-start(f32[8,4,1280]{2,1,0:T(4,128)} %fusion.6), calls=%async_computation.2 | async-start | bytes 327680 | tf_op jit(solution)/shard_map/all_to_all | solution.py:15
  45.5 0.0 copy-done.11
  45.6 0.0 copy-start.8
  45.6 4.0 %copy.53 = bf16[4,1024,256]{1,2,0:T(8,128)(2,1)} copy(bf16[4,1024,256]{2,1,0:T(8,128)(2,1)} %param.22) | data formatting | bytes 4194304 | tf_op args[2]
  49.6 0.0 copy-done.8
  49.6 0.1 iota_compare_fusion
  49.7 4.1 %all-to-all-done.2 = f32[8,4,1280]{2,1,0:T(4,128)S(1)} async-done(((f32[8,4,1280]{2,1,0:T(4,128)}), f32[8,4,1280]{2,1,0:T(4,128)S(1)}, u32[]{:S(2)}, u32[]{:S(2)}) %all-to-all-start.2) | async-done | bytes 163872 | tf_op jit(solution)/shard_map/all_to_all | solution.py:15
  53.8 0.1 fusion.43
  53.9 1.6 %select_reduce_fusion.2 = (f32[4,3]{1,0:T(4,128)S(1)}, f32[4,3,1024]{2,1,0:T(4,128)S(1)}) fusion(pred[4,1024]{1,0:T(4,128)(4,1)S(1)} %iota_compare_fusion, bf16[4,1024,1,2,128]{1,4,3,0,2:T(8,128)(2,1)} %bitcast.113, bf16[4,1,3,1,128]{4,0,3,2,1:T(4,128)(2,1)S(1)} %get-tuple-element.17), kind=kOutput, calls=%fused_computation.34 | convolution fusion | flops 3182580 | bytes 1104944 | tf_op jit(solution)/shard_map/sghd,scgd->sghc/dot_general | solution.py:46
  55.5 0.1 fusion.44
  55.6 1.6 %fusion.21 = (f32[4,3]{1,0:T(4,128)S(1)}, f32[4,3]{1,0:T(4,128)S(1)}, f32[4,3,1024]{2,1,0:T(4,128)S(1)}) fusion(f32[4,3,1024]{2,1,0:T(4,128)S(1)} %get-tuple-element.21, f32[4,3]{1,0:T(4,128)S(1)} %multiply_maximum_fusion.1, pred[4,1024]{1,0:T(4,128)(4,1)S(1)} %iota_compare_fusion, bf16[4,1024,1,2,128]{1,4,3,0,2:T(8,128)(2,1)} %bitcast.114, ...), kind=kOutput, calls=%fused_computation.36 | convolution fusion | flops 3219432 | bytes 1154192 | tf_op jit(solution)/shard_map/sghd,scgd->sghc/dot_general | solution.py:46
  57.2 0.2 fusion.22
  57.4 0.0 copy-done.9
  57.4 0.0 copy-done
  57.4 0.5 multiply_reduce_fusion.2
  58.0 0.0 copy-done.5
  58.0 0.1 fusion.41
  58.1 0.6 broadcast_in_dim.120
  58.7 3.3 %all-to-all-start.3 = ((bf16[8,4,768]{2,1,0:T(4,128)(2,1)}), bf16[8,4,768]{2,1,0:T(4,128)(2,1)S(1)}, u32[]{:S(2)}, u32[]{:S(2)}) async-start(bf16[8,4,768]{2,1,0:T(4,128)(2,1)} %broadcast_in_dim.120), calls=%async_computation.3 | async-start | bytes 98304 | tf_op jit(solution)/shard_map/all_to_all | solution.py:15
  62.1 0.0 copy-done.6
  62.1 6.9 %all-to-all-done.3 = bf16[8,4,768]{2,1,0:T(4,128)(2,1)S(1)} async-done(((bf16[8,4,768]{2,1,0:T(4,128)(2,1)}), bf16[8,4,768]{2,1,0:T(4,128)(2,1)S(1)}, u32[]{:S(2)}, u32[]{:S(2)}) %all-to-all-start.3) | async-done | bytes 49184 | tf_op jit(solution)/shard_map/all_to_all | solution.py:15
  69.1 0.2 convolution_convert_fusion.1
  69.3 0.1 broadcast_in_dim.121
  69.3 0.6 broadcast_in_dim.122
  70.0 8.5 %all-to-all-start.4 = ((bf16[16,4,256]{2,1,0:T(4,128)(2,1)}), bf16[16,4,256]{2,1,0:T(4,128)(2,1)S(1)}, u32[]{:S(2)}, u32[]{:S(2)}) async-start(bf16[16,4,256]{2,1,0:T(4,128)(2,1)} %bitcast.20), calls=%async_computation.4 | async-start | bytes 65536 | tf_op jit(solution)/shard_map/all_to_all | solution.py:15
  78.5 0.1 fusion.42
  78.6 0.1 copy.58
  78.7 7.3 %all-to-all-done.4 = bf16[16,4,256]{2,1,0:T(4,128)(2,1)S(1)} async-done(((bf16[16,4,256]{2,1,0:T(4,128)(2,1)}), bf16[16,4,256]{2,1,0:T(4,128)(2,1)S(1)}, u32[]{:S(2)}, u32[]{:S(2)}) %all-to-all-start.4) | async-done | bytes 32800 | tf_op jit(solution)/shard_map/all_to_all | solution.py:15
  86.0 0.0 copy-done.1
  86.0 0.0 copy-done.2
  86.1 0.2 convert_reduce_fusion.1
  86.3 0.2 fusion.28
  86.5 0.0 copy-done.3
  86.5 0.1 fusion.59
  86.6 1.0 select_reduce_fusion
  87.6 24.7 %all_to_all.36 = bf16[128,16,128]{2,1,0:T(8,128)(2,1)S(1)} all-to-all(bf16[128,16,128]{2,1,0:T(8,128)(2,1)S(1)} %select_reduce_fusion), channel_id=1, replica_groups=mesh['z'=8,'y'=4,'x'=4,'tp'=2] {'z','y','x'}, dimensions={0} | all-to-all | bytes 1048576 | tf_op jit(solution)/shard_map/all_to_all | solution.py:15
  112.3 1.5 %fusion.4 = f32[128,256]{1,0:T(8,128)S(1)} fusion(bf16[1,2048,256]{2,1,0:T(8,128)(2,1)} %param.36, bf16[16,8,16,128]{3,2,1,0:T(8,128)(2,1)S(1)} %bitcast.109), kind=kOutput, calls=%fused_computation.14 | convolution fusion | flops 134217728 | bytes 1703936 | tf_op jit(solution)/shard_map/dot_general | solution.py:154
  113.8 0.0 copy-start.7
  113.8 0.0 copy-start.10
  113.8 2.3 %convolution_convert_fusion = bf16[128,2048]{1,0:T(8,128)(2,1)S(1)} fusion(bf16[1,256,2048]{2,1,0:T(8,128)(2,1)} %param.38, bf16[1,2048,256]{2,1,0:T(8,128)(2,1)} %param.37, bf16[16,8,16,128]{3,2,1,0:T(8,128)(2,1)S(1)} %bitcast.110, f32[128,256]{1,0:T(8,128)S(1)} %fusion.4), kind=kOutput, calls=%fused_computation | convolution fusion | flops 268894208 | bytes 3276800 | tf_op jit(solution)/shard_map/dot_general | solution.py:157
  116.1 0.0 copy-start.4
  116.2 1.0 reshape.284
  117.2 7.5 %all-to-all-start.6 = ((bf16[256,8,128]{2,1,0:T(8,128)(2,1)}), bf16[256,8,128]{2,1,0:T(8,128)(2,1)S(1)}, u32[]{:S(2)}, u32[]{:S(2)}) async-start(bf16[256,8,128]{2,1,0:T(8,128)(2,1)} %reshape.284), calls=%async_computation.6 | async-start | bytes 1048576 | tf_op jit(solution)/shard_map/all_to_all | solution.py:15
  124.7 0.0 copy-done.7
  124.7 0.0 copy-done.10
  124.8 0.1 select_reduce_fusion.3
  124.8 0.1 fusion.30
  124.9 19.8 %all-to-all-done.6 = bf16[256,8,128]{2,1,0:T(8,128)(2,1)S(1)} async-done(((bf16[256,8,128]{2,1,0:T(8,128)(2,1)}), bf16[256,8,128]{2,1,0:T(8,128)(2,1)S(1)}, u32[]{:S(2)}, u32[]{:S(2)}) %all-to-all-start.6) | async-done | bytes 524320 | tf_op jit(solution)/shard_map/all_to_all | solution.py:15
  144.7 0.1 convert_reduce_fusion
  144.9 0.7 multiply_reduce_fusion
  145.6 0.2 fusion.54
  145.8 2.4 %all-gather.1 = f32[2,2,4]{2,1,0:T(2,128)S(1)} all-gather(f32[1,2,4]{2,1,0:T(2,128)S(1)} %maximum_bitcast_fusion), channel_id=2, replica_groups=mesh['z'=8,'y'=4,'x'=4,'tp'=2] {'tp'}, dimensions={0}, use_global_device_ids=true | all-gather | bytes 96 | tf_op jit(solution)/shard_map/all_gather | solution.py:169
  148.2 0.0 copy-done.4
  148.2 0.7 multiply_convert_fusion
  (33 shorter events, 0.3 us)
Async XLA Ops:
  0.0 57.4 %copy-start = (bf16[4,1024,256]{2,1,0:T(8,128)(2,1)S(1)}, bf16[4,1024,256]{2,1,0:T(8,128)(2,1)}, u32[]{:S(2)}) copy-start(bf16[4,1024,256]{2,1,0:T(8,128)(2,1)} %param.23) | copy-start | bytes 6291460
  3.3 15.6 %all-to-all-start = ((bf16[8,4,256]{2,1,0:T(4,128)(2,1)}), bf16[8,4,256]{2,1,0:T(4,128)(2,1)S(1)}, u32[]{:S(2)}, u32[]{:S(2)}) async-start(bf16[8,4,256]{2,1,0:T(4,128)(2,1)} %bitcast.1), calls=%async_computation | async-start | bytes 32768 | tf_op jit(solution)/shard_map/all_to_all | solution.py:15
  13.1 32.4 %copy-start.11 = (s32[4]{0:T(128)S(1)}, s32[4]{0:T(128)}, u32[]{:S(2)}) copy-start(s32[4]{0:T(128)} %param.32) | copy-start | bytes 52
  42.2 11.6 %all-to-all-start.2 = ((f32[8,4,1280]{2,1,0:T(4,128)}), f32[8,4,1280]{2,1,0:T(4,128)S(1)}, u32[]{:S(2)}, u32[]{:S(2)}) async-start(f32[8,4,1280]{2,1,0:T(4,128)} %fusion.6), calls=%async_computation.2 | async-start | bytes 327680 | tf_op jit(solution)/shard_map/all_to_all | solution.py:15
  45.6 4.0 %copy-start.8 = (s32[4]{0:T(128)S(1)}, s32[4]{0:T(128)}, u32[]{:S(2)}) copy-start(s32[4]{0:T(128)} %param.21) | copy-start | bytes 52
  49.6 7.8 %copy-start.9 = (f32[3]{0:T(128)S(1)}, f32[3]{0:T(128)}, u32[]{:S(2)}) copy-start(f32[3]{0:T(128)} %param.28) | copy-start | bytes 40
  55.5 2.5 %copy-start.5 = (f32[256]{0:T(256)S(1)}, f32[256]{0:T(256)}, u32[]{:S(2)}) copy-start(f32[256]{0:T(256)} %param.29) | copy-start | bytes 3076
  55.5 6.6 %copy-start.6 = (s32[4,2]{0,1:T(2,128)S(1)}, s32[4,2]{0,1:T(2,128)}, u32[]{:S(2)}) copy-start(s32[4,2]{0,1:T(2,128)} %param.33) | copy-start | bytes 100
  57.2 28.8 %copy-start.1 = (bf16[4,2048]{1,0:T(4,128)(2,1)S(1)}, bf16[4,2048]{1,0:T(4,128)(2,1)}, u32[]{:S(2)}) copy-start(bf16[4,2048]{1,0:T(4,128)(2,1)} %param.20) | copy-start | bytes 49156
  57.2 28.8 %copy-start.2 = (f32[2048]{0:T(1024)S(1)}, f32[2048]{0:T(1024)}, u32[]{:S(2)}) copy-start(f32[2048]{0:T(1024)} %param.24) | copy-start | bytes 24580
  57.2 29.3 %copy-start.3 = (f32[2048]{0:T(1024)S(1)}, f32[2048]{0:T(1024)}, u32[]{:S(2)}) copy-start(f32[2048]{0:T(1024)} %param.31) | copy-start | bytes 24580
  58.7 10.3 %all-to-all-start.3 = ((bf16[8,4,768]{2,1,0:T(4,128)(2,1)}), bf16[8,4,768]{2,1,0:T(4,128)(2,1)S(1)}, u32[]{:S(2)}, u32[]{:S(2)}) async-start(bf16[8,4,768]{2,1,0:T(4,128)(2,1)} %broadcast_in_dim.120), calls=%async_computation.3 | async-start | bytes 98304 | tf_op jit(solution)/shard_map/all_to_all | solution.py:15
  70.0 16.0 %all-to-all-start.4 = ((bf16[16,4,256]{2,1,0:T(4,128)(2,1)}), bf16[16,4,256]{2,1,0:T(4,128)(2,1)S(1)}, u32[]{:S(2)}, u32[]{:S(2)}) async-start(bf16[16,4,256]{2,1,0:T(4,128)(2,1)} %bitcast.20), calls=%async_computation.4 | async-start | bytes 65536 | tf_op jit(solution)/shard_map/all_to_all | solution.py:15
  113.8 10.9 %copy-start.7 = (f32[4,2]{0,1:T(2,128)S(1)}, f32[4,2]{0,1:T(2,128)}, u32[]{:S(2)}) copy-start(f32[4,2]{0,1:T(2,128)} %param.35) | copy-start | bytes 100
  113.8 10.9 %copy-start.10 = (f32[4]{0:T(128)S(1)}, f32[4]{0:T(128)}, u32[]{:S(2)}) copy-start(f32[4]{0:T(128)} %param.34) | copy-start | bytes 52
  116.1 32.0 %copy-start.4 = (f32[1024]{0:T(1024)S(1)}, f32[1024]{0:T(1024)}, u32[]{:S(2)}) copy-start(f32[1024]{0:T(1024)} %param.39) | copy-start | bytes 12292
  117.2 27.6 %all-to-all-start.6 = ((bf16[256,8,128]{2,1,0:T(8,128)(2,1)}), bf16[256,8,128]{2,1,0:T(8,128)(2,1)S(1)}, u32[]{:S(2)}, u32[]{:S(2)}) async-start(bf16[256,8,128]{2,1,0:T(8,128)(2,1)} %reshape.284), calls=%async_computation.6 | async-start | bytes 1048576 | tf_op jit(solution)/shard_map/all_to_all | solution.py:15
